TPU v7x, 512 devices: a whole 4x8x8 slice. The times are simulated.
512 devices in a mesh: sp: 64 (over z, y), tp: 8 (over x, core).
Axes of the slice: x: 4, y: 8, z: 8, core: 2. Of those that a mesh axis runs over, the one named last changes fastest.
Arguments:
- inner_pre: bfloat16 [24576, 4096], P('sp', 'tp'), may hold values from -6 to 6
- coeff_pre: bfloat16 [24576, 2, 1024], P('sp', None, 'tp'), may hold values from -6 to 6
- gate_pre: bfloat16 [24576, 4096], P('sp', 'tp'), may hold values from -6 to 6
- step_raw: bfloat16 [24576, 64], P('sp', 'tp'), may hold values from -2.5 to 2.5
- step_bias: float32 [64], P('tp'), may hold values from -3.3 to 0.8
- decay_log: float32 [64], P('tp'), may hold values from -8.5 to -3.5
- conv_inner: bfloat16 [4, 4096], P(None, 'tp'), may hold values from -3 to 3
- conv_coeff: bfloat16 [4, 2, 1024], P(None, None, 'tp'), may hold values from -3 to 3
- mixer_gain: float32 [4096], P('tp'), may hold values from 0.1 to 1.9
- out_weight: bfloat16 [4096, 2048], P('tp'), may hold values from -0.125 to 0.125
- residual: bfloat16 [24576, 2048], P('sp', 'tp'), may hold values from -12 to 12
- mlp_gain: float32 [2048], P('tp'), may hold values from 0.1 to 1.9
- up_weight: bfloat16 [2048, 8192], P('sp', 'tp'), may hold values from -0.125 to 0.125
- down_weight: bfloat16 [8192, 2048], P('tp', 'sp'), may hold values from -0.1875 to 0.1875
Outputs:
- layer_out: bfloat16 [24576, 2048], P('sp', 'tp')
All inputs are finite; a program needn't handle non-finite values.
Results may differ from a plain program's by a relative error of at most 0.02.
Values may be sent and summed in bfloat16 or wider, within the bound.
A program may use at most 64 MiB of HBM per device.

v0:
```python
import jax
import jax.numpy as jnp
from jax import lax
from jax.sharding import Mesh
from jax.sharding import PartitionSpec as P

D = 2048
INNER = 4096
HEAD_DIM = 64
GROUPS = 8
STATE = 128
BLOCK = 128
SP = ("sp_0", "sp_1")
eps_norm = 1e-05


def turned_gather(arrays, axis, dims):
    turned = [jnp.moveaxis(a, dim, 0) for a, dim in zip(arrays, dims)]
    both = jnp.concatenate([t.reshape(len(t), -1) for t in turned], axis=1)
    result, at, finished = (lax.all_gather(both, axis, axis=0, tiled=True), 0, [])
    for t, dim in zip(turned, dims):
        share = result[:, at : at + t[0].size].reshape(-1, *t.shape[1:])
        finished.append(jnp.moveaxis(share, 0, dim))
        at += t[0].size
    return tuple(finished)


def passed_along(block, axis, distance):
    devices = range(lax.axis_size(axis))
    route = [(i - distance, i) for i in devices if i - distance in devices]
    return lax.ppermute(block, axis, route)


def nothing_yet(array, identity):
    return jax.tree.map(
        lambda a, e: jnp.broadcast_to(jnp.asarray(e, a.dtype), a.shape), array, identity
    )


def carried_in(array, axes, combine, identity):
    before = start = nothing_yet(array, identity)
    so_far = array
    for axis in reversed(axes):
        size, index = (lax.axis_size(axis), lax.axis_index(axis))
        pieces = jax.tree.map(
            lambda part, kind: lax.all_gather(part.astype(kind), axis),
            so_far,
            (jnp.bfloat16, jnp.bfloat16),
        )
        inside, so_far = (start, start)
        for k in range(size):
            passed = k < index
            so_far = combine(
                so_far, jax.tree.map(lambda part, own: part[k].astype(own.dtype), pieces, array)
            )
            inside = jax.tree.map(lambda new, old: jnp.where(passed, new, old), so_far, inside)
        before = combine(inside, before)
    return before


def in_blocks(array, dim, size):
    before, after = (array.shape[:dim], array.shape[dim + 1 :])
    return jnp.moveaxis(array.reshape(*before, size, -1, *after), dim, 0)


def sent_and_summed(array, axis, dim):
    parts = in_blocks(array, dim, lax.axis_size(axis))
    arrived = lax.all_to_all(parts, axis, split_axis=0, concat_axis=0, tiled=True)
    return arrived.astype(jnp.float32).sum(axis=0)


def copy_for_each(array, axis):
    size = lax.axis_size(axis)
    return lax.all_to_all(
        jnp.broadcast_to(array[None], (size, *array.shape)), axis, 0, 0, tiled=True
    )


def of_everyone(array, axis):
    everything = copy_for_each(array, axis)
    return jnp.sum(everything, axis=0)


def laid_out(parts, dim):
    shape = list(parts.shape[1:])
    shape[dim] *= parts.shape[0]
    return jnp.moveaxis(parts, 0, dim).reshape(shape)


def gathered_copies(array, axis, dim):
    return laid_out(copy_for_each(array, axis), dim)


def causal_taps(history, current, weights):
    extended = jnp.concatenate([history, current], axis=0).astype(jnp.float32)
    length = current.shape[0]
    summed = extended[0:length] * weights[0].astype(jnp.float32)
    for offset in range(1, weights.shape[0]):
        summed = summed + extended[offset : offset + length] * weights[offset].astype(jnp.float32)
    return jax.nn.silu(summed)


def combine_states(first_part, second_part):
    decay_one, state_one = first_part
    decay_two, state_two = second_part
    return (decay_one * decay_two, state_one * decay_two[..., None, None] + state_two)


def shards(
    inner_pre,
    coeff_pre,
    gate_pre,
    step_raw,
    step_bias,
    decay_log,
    conv_inner,
    conv_coeff,
    mixer_gain,
    out_weight,
    residual,
    mlp_gain,
    up_weight,
    down_weight,
):
    up_whole, down_whole = turned_gather((up_weight, down_weight), SP, (0, 1))
    row_count = inner_pre.shape[0]
    edge_rows = conv_inner.shape[0] - 1
    inner_cols = inner_pre.shape[1]
    coeff_cols = coeff_pre.shape[2]
    tail_rows = jnp.concatenate(
        [
            inner_pre[row_count - edge_rows :],
            coeff_pre[row_count - edge_rows :].reshape(edge_rows, 2 * coeff_cols),
        ],
        axis=1,
    )
    arrived = passed_along(tail_rows, SP, 1)
    inner_act = causal_taps(arrived[:, :inner_cols], inner_pre, conv_inner)
    coeff_act = causal_taps(
        arrived[:, inner_cols:].reshape(edge_rows, 2, coeff_cols), coeff_pre, conv_coeff
    )
    heads_here = step_raw.shape[1]
    groups_here = coeff_cols // STATE
    per_group = heads_here // groups_here
    blocks = row_count // BLOCK
    in_coeff = coeff_act[:, 0].reshape(blocks, BLOCK, groups_here, STATE)
    out_coeff = coeff_act[:, 1].reshape(blocks, BLOCK, groups_here, STATE)
    step_size = jax.nn.softplus(step_raw.astype(jnp.float32) + step_bias)
    log_step = (-step_size * jnp.exp(decay_log)).reshape(blocks, BLOCK, groups_here, per_group)
    values = (
        inner_act.reshape(blocks, BLOCK, groups_here, per_group, HEAD_DIM)
        * step_size.reshape(blocks, BLOCK, groups_here, per_group)[..., None]
    )
    log_cumul = jnp.cumsum(log_step, axis=1)
    position = jnp.arange(BLOCK)
    causal_mask = (position[:, None] >= position[None, :])[None, :, :, None, None]
    log_gaps = log_cumul[:, :, None] - log_cumul[:, None, :]
    within = jnp.where(causal_mask, jnp.exp(jnp.where(causal_mask, log_gaps, 0.0)), 0.0)
    scores = jnp.einsum("blgn,bsgn->blsg", out_coeff, in_coeff)
    inside = jnp.einsum("blsg,blsgh,bsghp->blghp", scores, within, values)
    to_end = jnp.exp(log_cumul[:, -1:] - log_cumul)
    block_states = jnp.einsum("blgn,blgh,blghp->bghpn", in_coeff, to_end, values)
    block_logs = log_cumul[:, -1]
    block_ends = jnp.cumsum(block_logs, axis=0)
    block_starts = block_ends - block_logs
    block_index = jnp.arange(blocks)
    before = (block_index[None, :] < block_index[:, None])[:, :, None, None]
    log_spans = block_starts[:, None] - block_ends[None, :]
    block_links = jnp.where(before, jnp.exp(jnp.where(before, log_spans, 0.0)), 0.0)
    entering = jnp.einsum("nmgh,mghpk->nghpk", block_links, block_states)
    own_state = jnp.einsum(
        "mgh,mghpk->ghpk", jnp.exp(block_ends[-1][None] - block_ends), block_states
    )
    own_decay = jnp.exp(block_ends[-1])
    identity = (jnp.ones_like(own_decay), jnp.zeros_like(own_state))
    enter_decay, enter_state = carried_in((own_decay, own_state), SP, combine_states, identity)
    entering = entering + jnp.exp(block_starts)[..., None, None] * enter_state[None]
    carried = jnp.einsum("blgn,bghpn,blgh->blghp", out_coeff, entering, jnp.exp(log_cumul))
    scan_out = (inside + carried).reshape(row_count, inner_cols)
    gated = scan_out * jax.nn.silu(gate_pre.astype(jnp.float32))
    grouped = gated.reshape(row_count, groups_here, INNER // GROUPS)
    grouped = grouped * lax.rsqrt(jnp.mean(grouped * grouped, axis=2, keepdims=True) + eps_norm)
    mixed_rows = (grouped.reshape(row_count, inner_cols) * mixer_gain).astype(jnp.bfloat16)
    projected = sent_and_summed(
        jnp.dot(mixed_rows, out_weight, preferred_element_type=jnp.float32).astype(jnp.bfloat16),
        "tp",
        1,
    )
    first_sum = (residual.astype(jnp.float32) + projected).astype(jnp.bfloat16)
    first_wide = first_sum.astype(jnp.float32)
    squares = of_everyone(jnp.sum(first_wide * first_wide, axis=1), "tp")
    normed = (first_wide * lax.rsqrt(squares / D + eps_norm)[:, None] * mlp_gain).astype(
        jnp.bfloat16
    )
    whole_rows = gathered_copies(normed, "tp", 1)
    hidden = jnp.dot(whole_rows, up_whole, preferred_element_type=jnp.float32)
    active = jnp.square(jax.nn.relu(hidden)).astype(jnp.bfloat16)
    partials = jnp.dot(active, down_whole, preferred_element_type=jnp.float32)
    lowered = sent_and_summed(partials.astype(jnp.bfloat16), "tp", 1)
    return (first_wide + lowered).astype(jnp.bfloat16)


def solution(mesh):
    split = Mesh(mesh.devices.reshape(8, 8, mesh.shape["tp"]), ("sp_0", "sp_1", "tp"))
    return jax.shard_map(
        shards,
        mesh=split,
        in_specs=(
            P(SP, "tp"),
            P(SP, None, "tp"),
            P(SP, "tp"),
            P(SP, "tp"),
            P("tp"),
            P("tp"),
            P(None, "tp"),
            P(None, None, "tp"),
            P("tp"),
            P("tp", None),
            P(SP, "tp"),
            P("tp"),
            P(SP, "tp"),
            P("tp", SP),
        ),
        out_specs=P(SP, "tp"),
        check_vma=False,
    )
```

profile of v0, /device:TPU:1, one launch (start us, length us, event | category | flops | bytes accessed | tf_op | source)
XLA Modules:
  0.0 260.9 jit_solution(793769002312632758)
XLA Ops:
  6.5 0.9 slice.176
  7.4 0.7 slice_bitcast_fusion.8
  8.1 0.8 copy.96
  8.9 4.0 %collective-permute-start = (bf16[3,768]{0,1:T(8,128)(2,1)}, bf16[3,768]{0,1:T(8,128)(2,1)S(1)}, u32[]{:S(2)}, u32[]{:S(2)}) collective-permute-start(bf16[3,768]{0,1:T(8,128)(2,1)} %copy.96), channel_id=1, source_target_pairs={{0,8},{8,16},{16,24},{24,32},{32,40},{40,48},{48,56},{56,64},{64,7... | collective-permute-start | bytes 13832 | tf_op jit(solution)/shard_map/ppermute | solution.py:31
  13.0 0.7 exp.65
  13.6 0.8 fusion.70
  14.7 0.6 slice_bitcast_fusion.16
  15.3 0.6 bitcast_subtract_fusion
  15.9 0.8 slice_convert_fusion.3
  16.7 1.3 bitcast_convert_fusion.3
  18.1 0.7 fusion.99
  19.0 0.7 copy.106
  19.7 0.7 copy.122
  21.1 1.9 divide_multiply_fusion
  23.0 1.5 reshape.593
  24.6 1.1 maximum_convert_fusion.1
  25.8 0.6 divide_multiply_fusion.1
  26.7 1.1 broadcast_multiply_fusion
  28.9 0.7 convert_element_type.466
  29.7 13.0 %all_gather.21 = bf16[8,1,8]{2,1,0:T(2,128)(2,1)S(1)} all-gather(bf16[1,1,8]{2,1,0:T(2,128)(2,1)S(1)} %copy-done.52), channel_id=1, replica_groups=mesh['sp_0'=8,'sp_1'=8,'tp'=8] {'sp_1'}, dimensions={0}, use_global_device_ids=true | all-gather | bytes 144 | tf_op jit(solution)/shard_map/all_gather | solution.py:46
  43.2 26.5 %all-gather.9.cloned.1.call-done = bf16[64,64,128]{2,1,0:T(8,128)(2,1)} async-done(((bf16[8,64,128]{2,1,0:T(8,128)(2,1)}), bf16[64,64,128]{2,1,0:T(8,128)(2,1)}) %all-gather.9.cloned.1.call-update) | async-done | bytes 1048592 | tf_op jit(solution)/shard_map/all_gather | solution.py:46
  69.7 2.2 fusion.64
  72.1 0.7 pad_maximum_fusion
  72.8 0.7 copy.100
  73.5 0.7 copy.112
  74.2 0.7 copy.125
  74.8 0.7 copy.110
  75.6 1.0 copy.115
  76.6 13.6 %all_gather.22 = bf16[8,1,8]{2,1,0:T(2,128)(2,1)S(1)} all-gather(bf16[1,1,8]{2,1,0:T(2,128)(2,1)S(1)} %multiply_convert_fusion.3), channel_id=1, replica_groups=mesh['sp_0'=8,'sp_1'=8,'tp'=8] {'sp_0'}, dimensions={0}, use_global_device_ids=true | all-gather | bytes 144 | tf_op jit(solution)/shard_map/all_gather | solution.py:46
  90.2 0.6 iota_compare_fusion.1
  90.8 0.6 iota_compare_fusion
  91.9 0.6 fusion.83
  92.8 0.8 copy.98
  93.7 2.8 %fusion.17 = f32[3,128,1,8,64]{1,4,3,0,2:T(8,128)} fusion(bf16[3,128,8,64]{1,0,3,2:T(4,128)(2,1)} %get-tuple-element.8, f32[3,128,8]{1,2,0:T(8,128)} %copy.100, f32[3,128,128]{2,1,0:T(8,128)} %copy.98, pred[128,128]{1,0:T(8,128)(4,1)} %iota_compare_fusion), kind=kOutput, calls=%fused_computation.20 | convolution fusion | flops 51904512 | bytes 1404928 | tf_op jit(solution)/shard_map/blsg,blsgh,bsghp->blghp/dot_general | solution.py:160
  96.6 16.6 %all-gather.5.cloned.1.call-done = bf16[8,1,8,64,128]{4,3,2,1,0:T(8,128)(2,1)} async-done(((bf16[1,1,8,64,128]{4,3,2,1,0:T(8,128)(2,1)}), bf16[8,1,8,64,128]{4,3,2,1,0:T(8,128)(2,1)}) %all-gather.5.cloned.1.call-update) | async-done | bytes 1048592 | tf_op jit(solution)/shard_map/all_gather | solution.py:46
  113.4 2.0 fusion.63
  115.4 0.6 fusion.16
  116.8 0.5 copy.114
  117.8 1.2 convolution_convert_fusion
  119.1 29.9 %all_to_all.21 = bf16[8,384,256]{2,1,0:T(8,128)(2,1)S(1)} all-to-all(bf16[8,384,256]{2,1,0:T(8,128)(2,1)S(1)} %bitcast.260), channel_id=1, replica_groups=mesh['sp_0'=8,'sp_1'=8,'tp'=8] {'tp'}, dimensions={0} | all-to-all | bytes 3145728 | tf_op jit(solution)/shard_map/all_to_all | solution.py:68
  149.3 0.7 copy-done.12
  150.1 8.0 %all_to_all.22 = f32[8,1,384]{2,1,0:T(1,128)S(1)} all-to-all(f32[8,1,384]{2,1,0:T(1,128)S(1)} %broadcast_in_dim.53), channel_id=1, replica_groups=mesh['sp_0'=8,'sp_1'=8,'tp'=8] {'tp'}, dimensions={0} | all-to-all | bytes 24576 | tf_op jit(solution)/shard_map/all_to_all | solution.py:74
  158.7 24.4 %all_to_all.23 = bf16[8,384,256]{1,2,0:T(8,128)(2,1)} all-to-all(bf16[8,384,256]{1,2,0:T(8,128)(2,1)S(1)} %broadcast_in_dim.54), channel_id=1, replica_groups=mesh['sp_0'=8,'sp_1'=8,'tp'=8] {'tp'}, dimensions={0} | all-to-all | bytes 3145728 | tf_op jit(solution)/shard_map/all_to_all | solution.py:74
  183.1 34.8 %all-gather.7.cloned.1.call-done = bf16[2048,2048]{1,0:T(8,128)(2,1)} async-done(((bf16[32,2048]{1,0:T(8,128)(2,1)}), bf16[2048,2048]{1,0:T(8,128)(2,1)}) %all-gather.7.cloned.1.call-update) | async-done | bytes 8388624 | tf_op jit(solution)/shard_map/all_gather | solution.py:20
  217.9 8.5 %fusion.4 = bf16[384,2048]{1,0:T(8,128)(2,1)} fusion(bf16[2048,2048]{1,0:T(8,128)(2,1)} %all-gather.7.cloned.1.call-done, bf16[384,2048]{0,1:T(8,128)(2,1)} %bitcast.270), kind=kOutput, calls=%fused_computation.6 | convolution fusion | flops 3223191552 | bytes 11534336 | tf_op jit(solution)/shard_map/dot_general | solution.py:198
  226.4 1.5 copy.160
  227.9 25.5 %all_to_all.24 = bf16[8,384,256]{2,1,0:T(8,128)(2,1)S(1)} all-to-all(bf16[8,384,256]{2,1,0:T(8,128)(2,1)S(1)} %bitcast.261), channel_id=1, replica_groups=mesh['sp_0'=8,'sp_1'=8,'tp'=8] {'tp'}, dimensions={0} | all-to-all | bytes 3145728 | tf_op jit(solution)/shard_map/all_to_all | solution.py:68
  253.7 0.7 fusion.47
  (156 shorter events, 6.5 us)
Async XLA Ops:
  6.5 111.3 %copy-start = (bf16[512,2048]{1,0:T(8,128)(2,1)S(1)}, bf16[512,2048]{1,0:T(8,128)(2,1)}, u32[]{:S(2)}) copy-start(bf16[512,2048]{1,0:T(8,128)(2,1)} %param.23) | copy-start | bytes 6291460
  6.5 12.3 %copy-start.7 = (bf16[384,512]{1,0:T(8,128)(2,1)S(1)}, bf16[384,512]{1,0:T(8,128)(2,1)}, u32[]{:S(2)}) copy-start(bf16[384,512]{1,0:T(8,128)(2,1)} %param.14) | copy-start | bytes 1179652
  6.5 63.2 %all-gather.9.cloned.1.call-start = ((), (), s32[]{:S(2)}) async-start(), calls=%async_computation.6 | async-start | bytes 1179648 | tf_op jit(solution)/shard_map/all_gather | solution.py:46
  8.9 11.5 %collective-permute-start = (bf16[3,768]{0,1:T(8,128)(2,1)}, bf16[3,768]{0,1:T(8,128)(2,1)S(1)}, u32[]{:S(2)}, u32[]{:S(2)}) collective-permute-start(bf16[3,768]{0,1:T(8,128)(2,1)} %copy.96), channel_id=1, source_target_pairs={{0,8},{8,16},{16,24},{24,32},{32,40},{40,48},{48,56},{56,64},{64,7... | collective-permute-start | bytes 13832 | tf_op jit(solution)/shard_map/ppermute | solution.py:31
  14.7 4.1 %copy-start.16 = (f32[3,1,8]{2,1,0:T(1,128)}, f32[3,1,8]{2,1,0:T(1,128)S(1)}, u32[]{:S(2)}) copy-start(f32[3,1,8]{2,1,0:T(1,128)S(1)} %fusion.75) | copy-start | bytes 292
  23.0 2.7 %copy-start.35 = (f32[2,128]{1,0:T(2,128)S(1)}, f32[2,128]{1,0:T(2,128)}, u32[]{:S(2)}) copy-start(f32[2,128]{1,0:T(2,128)} %get-tuple-element.37) | copy-start | bytes 3076
  23.0 2.7 %copy-start.36 = (f32[2,128]{1,0:T(2,128)S(1)}, f32[2,128]{1,0:T(2,128)}, u32[]{:S(2)}) copy-start(f32[2,128]{1,0:T(2,128)} %get-tuple-element.38) | copy-start | bytes 3076
  23.0 2.7 %copy-start.37 = (f32[2,128]{1,0:T(2,128)S(1)}, f32[2,128]{1,0:T(2,128)}, u32[]{:S(2)}) copy-start(f32[2,128]{1,0:T(2,128)} %get-tuple-element.39) | copy-start | bytes 3076
  23.0 2.7 %copy-start.38 = (f32[2,128]{1,0:T(2,128)S(1)}, f32[2,128]{1,0:T(2,128)}, u32[]{:S(2)}) copy-start(f32[2,128]{1,0:T(2,128)} %get-tuple-element.40) | copy-start | bytes 3076
  28.1 43.9 %copy-start.14 = (bf16[1024,32]{0,1:T(8,128)(2,1)S(1)}, bf16[1024,32]{0,1:T(8,128)(2,1)}, u32[]{:S(2)}) copy-start(bf16[1024,32]{0,1:T(8,128)(2,1)} %param.27) | copy-start | bytes 196612
  28.2 43.9 %copy-start.15 = (bf16[32,1024]{1,0:T(8,128)(2,1)S(1)}, bf16[32,1024]{1,0:T(8,128)(2,1)}, u32[]{:S(2)}) copy-start(bf16[32,1024]{1,0:T(8,128)(2,1)} %param.26) | copy-start | bytes 196612
  28.2 44.6 %copy-start.17 = (f32[3,1,8]{2,1,0:T(1,128)S(1)}, f32[3,1,8]{2,1,0:T(1,128)}, u32[]{:S(2)}) copy-start(f32[3,1,8]{2,1,0:T(1,128)} %copy-done.16) | copy-start | bytes 292
  28.2 45.3 %copy-start.19 = (f32[3,1,1,8]{3,2,1,0:T(1,128)S(1)}, f32[3,1,1,8]{3,2,1,0:T(1,128)}, u32[]{:S(2)}) copy-start(f32[3,1,1,8]{3,2,1,0:T(1,128)} %copy-done.18) | copy-start | bytes 292
  28.2 46.0 %copy-start.20 = (f32[3,1,1,8]{3,2,1,0:T(1,128)S(1)}, f32[3,1,1,8]{3,2,1,0:T(1,128)}, u32[]{:S(2)}) copy-start(f32[3,1,1,8]{3,2,1,0:T(1,128)} %get-tuple-element.13) | copy-start | bytes 292
  28.2 47.3 %copy-start.6 = (f32[3,128,8]{2,1,0:T(8,128)S(1)}, f32[3,128,8]{2,1,0:T(8,128)}, u32[]{:S(2)}) copy-start(f32[3,128,8]{2,1,0:T(8,128)} %get-tuple-element.11) | copy-start | bytes 36868
  28.7 46.9 %copy-start.8 = (bf16[384,512]{1,0:T(8,128)(2,1)S(1)}, bf16[384,512]{1,0:T(8,128)(2,1)}, u32[]{:S(2)}) copy-start(bf16[384,512]{1,0:T(8,128)(2,1)} %param.16) | copy-start | bytes 1179652
  29.6 62.9 %copy-start.3 = (f32[384,1,128]{2,1,0:T(1,128)S(1)}, f32[384,1,128]{2,1,0:T(1,128)}, u32[]{:S(2)}) copy-start(f32[384,1,128]{2,1,0:T(1,128)} %copy-done.2) | copy-start | bytes 589828
  29.6 83.6 %all-gather.5.cloned.1.call-start = ((), (), s32[]{:S(2)}) async-start(), calls=%async_computation.4 | async-start | bytes 1179648 | tf_op jit(solution)/shard_map/all_gather | solution.py:46
  43.2 49.5 %copy-start.33 = (f32[8]{0:T(128)}, f32[8]{0:T(128)S(1)}, u32[]{:S(2)}) copy-start(f32[8]{0:T(128)S(1)} %get-tuple-element.25) | copy-start | bytes 100
  43.2 49.5 %copy-start.21 = (f32[8]{0:T(128)}, f32[8]{0:T(128)S(1)}, u32[]{:S(2)}) copy-start(f32[8]{0:T(128)S(1)} %get-tuple-element.27) | copy-start | bytes 100
  43.2 49.5 %copy-start.23 = (f32[8]{0:T(128)}, f32[8]{0:T(128)S(1)}, u32[]{:S(2)}) copy-start(f32[8]{0:T(128)S(1)} %get-tuple-element.28) | copy-start | bytes 100
  43.2 49.5 %copy-start.25 = (f32[8]{0:T(128)}, f32[8]{0:T(128)S(1)}, u32[]{:S(2)}) copy-start(f32[8]{0:T(128)S(1)} %get-tuple-element.29) | copy-start | bytes 100
  43.2 49.5 %copy-start.27 = (f32[8]{0:T(128)}, f32[8]{0:T(128)S(1)}, u32[]{:S(2)}) copy-start(f32[8]{0:T(128)S(1)} %get-tuple-element.30) | copy-start | bytes 100
  43.2 49.5 %copy-start.29 = (f32[8]{0:T(128)}, f32[8]{0:T(128)S(1)}, u32[]{:S(2)}) copy-start(f32[8]{0:T(128)S(1)} %get-tuple-element.31) | copy-start | bytes 100
  43.2 49.5 %copy-start.31 = (f32[8]{0:T(128)}, f32[8]{0:T(128)S(1)}, u32[]{:S(2)}) copy-start(f32[8]{0:T(128)S(1)} %get-tuple-element.32) | copy-start | bytes 100
  72.0 145.9 %all-gather.7.cloned.1.call-start = ((), (), s32[]{:S(2)}) async-start(), calls=%async_computation.5 | async-start | bytes 8519680 | tf_op jit(solution)/shard_map/all_gather | solution.py:20
  93.6 19.6 %copy-start.1 = (bf16[64,64,128]{2,1,0:T(8,128)(2,1)S(1)}, bf16[64,64,128]{2,1,0:T(8,128)(2,1)}, u32[]{:S(2)}) copy-start(bf16[64,64,128]{2,1,0:T(8,128)(2,1)} %all-gather.9.cloned.1.call-done) | copy-start | bytes 3145732
  93.6 19.6 %copy-start.22 = (f32[8]{0:T(128)S(1)}, f32[8]{0:T(128)}, u32[]{:S(2)}) copy-start(f32[8]{0:T(128)} %copy-done.21) | copy-start | bytes 100
  93.6 19.6 %copy-start.24 = (f32[8]{0:T(128)S(1)}, f32[8]{0:T(128)}, u32[]{:S(2)}) copy-start(f32[8]{0:T(128)} %copy-done.23) | copy-start | bytes 100
  93.6 19.6 %copy-start.26 = (f32[8]{0:T(128)S(1)}, f32[8]{0:T(128)}, u32[]{:S(2)}) copy-start(f32[8]{0:T(128)} %copy-done.25) | copy-start | bytes 100
  93.6 19.6 %copy-start.28 = (f32[8]{0:T(128)S(1)}, f32[8]{0:T(128)}, u32[]{:S(2)}) copy-start(f32[8]{0:T(128)} %copy-done.27) | copy-start | bytes 100
  93.6 19.6 %copy-start.30 = (f32[8]{0:T(128)S(1)}, f32[8]{0:T(128)}, u32[]{:S(2)}) copy-start(f32[8]{0:T(128)} %copy-done.29) | copy-start | bytes 100
  93.6 19.6 %copy-start.32 = (f32[8]{0:T(128)S(1)}, f32[8]{0:T(128)}, u32[]{:S(2)}) copy-start(f32[8]{0:T(128)} %copy-done.31) | copy-start | bytes 100
  93.6 19.6 %copy-start.34 = (f32[8]{0:T(128)S(1)}, f32[8]{0:T(128)}, u32[]{:S(2)}) copy-start(f32[8]{0:T(128)} %copy-done.33) | copy-start | bytes 100
  93.6 19.6 %copy-start.43 = (f32[8]{0:T(128)S(1)}, f32[8]{0:T(128)}, u32[]{:S(2)}) copy-start(f32[8]{0:T(128)} %get-tuple-element.17) | copy-start | bytes 100
  93.6 19.6 %copy-start.44 = (f32[8]{0:T(128)S(1)}, f32[8]{0:T(128)}, u32[]{:S(2)}) copy-start(f32[8]{0:T(128)} %get-tuple-element.18) | copy-start | bytes 100
  93.7 19.6 %copy-start.45 = (f32[8]{0:T(128)S(1)}, f32[8]{0:T(128)}, u32[]{:S(2)}) copy-start(f32[8]{0:T(128)} %get-tuple-element.19) | copy-start | bytes 100
  93.7 19.6 %copy-start.46 = (f32[8]{0:T(128)S(1)}, f32[8]{0:T(128)}, u32[]{:S(2)}) copy-start(f32[8]{0:T(128)} %get-tuple-element.20) | copy-start | bytes 100
  93.7 19.6 %copy-start.47 = (f32[8]{0:T(128)S(1)}, f32[8]{0:T(128)}, u32[]{:S(2)}) copy-start(f32[8]{0:T(128)} %get-tuple-element.21) | copy-start | bytes 100
  93.7 19.6 %copy-start.48 = (f32[8]{0:T(128)S(1)}, f32[8]{0:T(128)}, u32[]{:S(2)}) copy-start(f32[8]{0:T(128)} %get-tuple-element.22) | copy-start | bytes 100
  93.7 19.6 %copy-start.49 = (f32[8]{0:T(128)S(1)}, f32[8]{0:T(128)}, u32[]{:S(2)}) copy-start(f32[8]{0:T(128)} %get-tuple-element.23) | copy-start | bytes 100
  93.7 19.6 %copy-start.50 = (f32[8]{0:T(128)S(1)}, f32[8]{0:T(128)}, u32[]{:S(2)}) copy-start(f32[8]{0:T(128)} %get-tuple-element.24) | copy-start | bytes 100
  93.7 19.6 %copy-start.53 = (f32[8]{0:T(128)S(1)}, f32[8]{0:T(128)}, u32[]{:S(2)}) copy-start(f32[8]{0:T(128)} %fusion.85) | copy-start | bytes 100
  96.6 18.8 %copy-start.40 = (f32[3,8]{0,1:T(8,128)S(1)}, f32[3,8]{0,1:T(8,128)}, u32[]{:S(2)}) copy-start(f32[3,8]{0,1:T(8,128)} %copy.112) | copy-start | bytes 292
  96.6 18.8 %copy-start.41 = (f32[3,8]{0,1:T(8,128)S(1)}, f32[3,8]{0,1:T(8,128)}, u32[]{:S(2)}) copy-start(f32[3,8]{0,1:T(8,128)} %copy.110) | copy-start | bytes 292
  96.6 18.9 %copy-start.42 = (f32[3,1,1,8]{0,3,2,1:T(8,128)S(1)}, f32[3,1,1,8]{0,3,2,1:T(8,128)}, u32[]{:S(2)}) copy-start(f32[3,1,1,8]{0,3,2,1:T(8,128)} %copy.125) | copy-start | bytes 292
  96.6 18.9 %copy-start.55 = (pred[3,3]{1,0:T(4,128)(4,1)S(1)}, pred[3,3]{1,0:T(4,128)(4,1)}, u32[]{:S(2)}) copy-start(pred[3,3]{1,0:T(4,128)(4,1)} %iota_compare_fusion.1) | copy-start | bytes 31
  149.0 9.2 %copy-start.51 = (f32[256]{0:T(256)S(1)}, f32[256]{0:T(256)}, u32[]{:S(2)}) copy-start(f32[256]{0:T(256)} %param.25) | copy-start | bytes 3076
  (13 other events, 18.7 us)
Sparse Core Ops, SparseCore 0:
  29.7 39.9 all-gather.8
  72.1 41.0 all-gather.4
  116.3 101.5 all-gather.6
where the time goes:
time: 262 us; the launch traced here: 261 us
  blocking collectives  115 us (44%)
  waiting for transfers between devices  78 us (30%)
  other arithmetic  20.3 us (8%)
  local copies, waits for them, and re-layouts  15.8 us (6%)
  matrix products  14.2 us (5%)
  between operations  14 us (5%)
  starting transfers between devices  4.1 us (2%)
    all_to_all x2, blocking collectives, sent_and_summed(): lax.all_to_all(parts, axis, split_axis=0, concat_axis=0, tiled=True)  55.5 us
    all_gather x2, waiting for transfers between devices, carried_in(): lax.all_gather(part.astype(kind), axis)  43.1 us
    all_gather x1, waiting for transfers between devices, turned_gather(): lax.all_gather(both, axis, axis=0, tiled=True)  34.8 us
    all_to_all x2, blocking collectives, copy_for_each(): lax.all_to_all(jnp.broadcast_to(array[None], (size, *array.shape)), axis,...  32.4 us
    all_gather x2, blocking collectives, carried_in(): lax.all_gather(part.astype(kind), axis)  26.6 us
    dot_general x1, matrix products, shards(): partials = jnp.dot(active, down_whole, preferred_element_type=jnp.float32)  8.49 us
  transfers between devices with their start and end apart: 4, of which 3 were waited for; matrix products, arithmetic and copies ran while one was open for 9% of the time, Pallas kernels for 0%

commit v1 on v0

--- a/solution.py
+++ b/solution.py
@@ -17,7 +17,16 @@
 def turned_gather(arrays, axis, dims):
     turned = [jnp.moveaxis(a, dim, 0) for a, dim in zip(arrays, dims)]
     both = jnp.concatenate([t.reshape(len(t), -1) for t in turned], axis=1)
-    result, at, finished = (lax.all_gather(both, axis, axis=0, tiled=True), 0, [])
+    result, at, finished = (
+        jnp.concatenate(
+            lax.all_to_all(
+                jnp.stack(lax.axis_size(axis) * [both]), axis_name=axis, split_axis=0, concat_axis=0
+            ),
+            axis=0,
+        ),
+        0,
+        [],
+    )
     for t, dim in zip(turned, dims):
         share = result[:, at : at + t[0].size].reshape(-1, *t.shape[1:])
         finished.append(jnp.moveaxis(share, 0, dim))

time: 262 us -> 440 us (1.68)
  the two profiles are of different devices: /device:TPU:1 before, /device:TPU:24 now
where the time goes in v1:
time: 440 us; the launch traced here: 439 us
  blocking collectives  299 us (68%)
  waiting for transfers between devices  65.1 us (15%)
  other arithmetic  19.7 us (4%)
  local copies, waits for them, and re-layouts  17.8 us (4%)
  matrix products  14.2 us (3%)
  between operations  14 us (3%)
  starting transfers between devices  9.36 us (2%)
    all_to_all x1, blocking collectives, turned_gather(): lax.all_to_all(jnp.stack(lax.axis_size(axis) * [both]), axis_name=axis, s...  211 us
    all_to_all x2, blocking collectives, sent_and_summed(): lax.all_to_all(parts, axis, split_axis=0, concat_axis=0, tiled=True)  49.7 us
    all_gather x2, waiting for transfers between devices, carried_in(): lax.all_gather(part.astype(kind), axis)  43.8 us
    all_gather x2, blocking collectives, carried_in(): lax.all_gather(part.astype(kind), axis)  30.4 us
    all_to_all x1, waiting for transfers between devices, copy_for_each(): lax.all_to_all(jnp.broadcast_to(array[None], (size, *array.shape)), axis,...  21.3 us
  transfers between devices with their start and end apart: 4, of which 3 were waited for; matrix products, arithmetic and copies ran while one was open for 4% of the time, Pallas kernels for 0%

profile of v1, /device:TPU:24, one launch (start us, length us, event | category | flops | bytes accessed | tf_op | source)
XLA Modules:
  0.0 439.2 jit_solution(15716794392138778103)
XLA Ops:
  6.5 0.8 slice_bitcast_fusion.8
  7.4 0.7 slice.176
  8.1 0.8 copy.96
  8.9 4.7 %collective-permute-start = (bf16[3,768]{0,1:T(8,128)(2,1)}, bf16[3,768]{0,1:T(8,128)(2,1)S(1)}, u32[]{:S(2)}, u32[]{:S(2)}) collective-permute-start(bf16[3,768]{0,1:T(8,128)(2,1)} %copy.96), channel_id=1, source_target_pairs={{0,8},{8,16},{16,24},{24,32},{32,40},{40,48},{48,56},{56,64},{64,7... | collective-permute-start | bytes 13832 | tf_op jit(solution)/shard_map/ppermute | solution.py:40
  13.6 0.7 exp.65
  14.3 0.8 fusion.70
  15.4 0.6 bitcast_subtract_fusion
  16.5 0.8 slice_convert_fusion.3
  17.4 1.3 bitcast_convert_fusion.3
  18.7 0.7 fusion.99
  19.7 0.7 copy.106
  20.4 0.7 copy.122
  21.7 1.9 divide_multiply_fusion
  23.6 1.5 reshape.598
  25.2 1.1 maximum_convert_fusion.1
  26.4 0.6 divide_multiply_fusion.1
  27.4 1.1 broadcast_multiply_fusion
  28.8 0.7 copy-done.9
  30.0 0.7 convert_element_type.466
  30.8 13.4 %all_gather.18 = bf16[8,1,8]{2,1,0:T(2,128)(2,1)S(1)} all-gather(bf16[1,1,8]{2,1,0:T(2,128)(2,1)S(1)} %copy-done.37), channel_id=1, replica_groups=mesh['sp_0'=8,'sp_1'=8,'tp'=8] {'sp_1'}, dimensions={0}, use_global_device_ids=true | all-gather | bytes 144 | tf_op jit(solution)/shard_map/all_gather | solution.py:55
  44.7 29.1 %all-gather.6.cloned.1.call-done = bf16[64,64,128]{2,1,0:T(8,128)(2,1)} async-done(((bf16[8,64,128]{2,1,0:T(8,128)(2,1)}), bf16[64,64,128]{2,1,0:T(8,128)(2,1)}) %all-gather.6.cloned.1.call-update) | async-done | bytes 1048592 | tf_op jit(solution)/shard_map/all_gather | solution.py:55
  73.9 2.3 fusion.64
  76.1 0.7 copy.100
  76.8 0.9 copy.115
  77.8 0.7 copy.112
  78.5 0.7 copy.110
  79.1 0.7 copy.125
  79.9 17.1 %all_gather.19 = bf16[8,1,8]{2,1,0:T(2,128)(2,1)S(1)} all-gather(bf16[1,1,8]{2,1,0:T(2,128)(2,1)S(1)} %multiply_convert_fusion.3), channel_id=1, replica_groups=mesh['sp_0'=8,'sp_1'=8,'tp'=8] {'sp_0'}, dimensions={0}, use_global_device_ids=true | all-gather | bytes 144 | tf_op jit(solution)/shard_map/all_gather | solution.py:55
  97.5 0.6 iota_compare_fusion
  98.1 0.6 fusion.85
  98.7 0.6 fusion.83
  99.8 2.8 fusion.17
  102.6 14.6 %all-gather.4.cloned.1.call-done = bf16[8,1,8,64,128]{4,3,2,1,0:T(8,128)(2,1)} async-done(((bf16[1,1,8,64,128]{4,3,2,1,0:T(8,128)(2,1)}), bf16[8,1,8,64,128]{4,3,2,1,0:T(8,128)(2,1)}) %all-gather.4.cloned.1.call-update) | async-done | bytes 1048592 | tf_op jit(solution)/shard_map/all_gather | solution.py:55
  117.2 2.1 fusion.63
  119.3 0.6 fusion.16
  121.7 1.2 convolution_convert_fusion
  123.0 25.6 %all_to_all.26 = bf16[8,384,256]{2,1,0:T(8,128)(2,1)S(1)} all-to-all(bf16[8,384,256]{2,1,0:T(8,128)(2,1)S(1)} %bitcast.262), channel_id=1, replica_groups=mesh['sp_0'=8,'sp_1'=8,'tp'=8] {'tp'}, dimensions={0} | all-to-all | bytes 3145728 | tf_op jit(solution)/shard_map/all_to_all | solution.py:77
  148.9 0.7 copy-done.12
  149.7 7.7 %all_to_all.27 = f32[8,1,384]{2,1,0:T(1,128)S(1)} all-to-all(f32[8,1,384]{2,1,0:T(1,128)S(1)} %broadcast_in_dim.53), channel_id=1, replica_groups=mesh['sp_0'=8,'sp_1'=8,'tp'=8] {'tp'}, dimensions={0} | all-to-all | bytes 24576 | tf_op jit(solution)/shard_map/all_to_all | solution.py:83
  157.8 1.3 broadcast_in_dim.54
  159.1 4.6 %all-to-all-start.2 = ((bf16[8,384,256]{1,2,0:T(8,128)(2,1)}), bf16[8,384,256]{1,2,0:T(8,128)(2,1)}, u32[]{:S(2)}, u32[]{:S(2)}) async-start(bf16[8,384,256]{1,2,0:T(8,128)(2,1)} %broadcast_in_dim.54), calls=%async_computation.2 | async-start | bytes 3145728 | tf_op jit(solution)/shard_map/all_to_all | solution.py:83
  163.8 21.3 %all-to-all-done.2 = bf16[8,384,256]{1,2,0:T(8,128)(2,1)} async-done(((bf16[8,384,256]{1,2,0:T(8,128)(2,1)}), bf16[8,384,256]{1,2,0:T(8,128)(2,1)}, u32[]{:S(2)}, u32[]{:S(2)}) %all-to-all-start.2) | async-done | bytes 1572896 | tf_op jit(solution)/shard_map/all_to_all | solution.py:83
  185.1 1.1 stack.2
  186.2 211.2 %all_to_all.28 = bf16[64,32,2048]{2,1,0:T(8,128)(2,1)} all-to-all(bf16[64,32,2048]{2,1,0:T(8,128)(2,1)S(1)} %stack.2), channel_id=1, replica_groups=mesh['sp_0'=8,'sp_1'=8,'tp'=8] {'sp_0','sp_1'}, dimensions={0} | all-to-all | bytes 16777216 | tf_op jit(solution)/shard_map/all_to_all | solution.py:22
  397.4 8.5 %fusion.4 = bf16[384,2048]{1,0:T(8,128)(2,1)} fusion(bf16[2048,2048]{1,0:T(8,128)(2,1)} %bitcast.261, bf16[384,2048]{0,1:T(8,128)(2,1)} %bitcast.64), kind=kOutput, calls=%fused_computation.6 | convolution fusion | flops 3223191552 | bytes 11534336 | tf_op jit(solution)/shard_map/dot_general | solution.py:207
  405.9 1.5 copy.160
  407.4 24.0 %all_to_all.29 = bf16[8,384,256]{2,1,0:T(8,128)(2,1)S(1)} all-to-all(bf16[8,384,256]{2,1,0:T(8,128)(2,1)S(1)} %bitcast.263), channel_id=1, replica_groups=mesh['sp_0'=8,'sp_1'=8,'tp'=8] {'tp'}, dimensions={0} | all-to-all | bytes 3145728 | tf_op jit(solution)/shard_map/all_to_all | solution.py:77
  431.7 0.7 fusion.47
  (124 shorter events, 7.3 us)
Async XLA Ops:
  6.5 115.2 %copy-start = (bf16[512,2048]{1,0:T(8,128)(2,1)S(1)}, bf16[512,2048]{1,0:T(8,128)(2,1)}, u32[]{:S(2)}) copy-start(bf16[512,2048]{1,0:T(8,128)(2,1)} %param.23) | copy-start | bytes 6291460
  6.5 12.9 %copy-start.7 = (bf16[384,512]{1,0:T(8,128)(2,1)S(1)}, bf16[384,512]{1,0:T(8,128)(2,1)}, u32[]{:S(2)}) copy-start(bf16[384,512]{1,0:T(8,128)(2,1)} %param.14) | copy-start | bytes 1179652
  6.5 67.3 %all-gather.6.cloned.1.call-start = ((), (), s32[]{:S(2)}) async-start(), calls=%async_computation.6 | async-start | bytes 1179648 | tf_op jit(solution)/shard_map/all_gather | solution.py:55
  8.9 12.1 %collective-permute-start = (bf16[3,768]{0,1:T(8,128)(2,1)}, bf16[3,768]{0,1:T(8,128)(2,1)S(1)}, u32[]{:S(2)}, u32[]{:S(2)}) collective-permute-start(bf16[3,768]{0,1:T(8,128)(2,1)} %copy.96), channel_id=1, source_target_pairs={{0,8},{8,16},{16,24},{24,32},{32,40},{40,48},{48,56},{56,64},{64,7... | collective-permute-start | bytes 13832 | tf_op jit(solution)/shard_map/ppermute | solution.py:40
  15.4 4.0 copy-start.16
  16.0 3.4 copy-start.18
  21.0 0.7 copy-start.11
  23.6 1.5 slice-start
  23.6 2.7 copy-start.28
  23.6 2.7 copy-start.29
  23.6 2.7 copy-start.30
  23.6 2.7 copy-start.31
  25.2 2.1 copy-start.13
  27.3 2.6 copy-start.2
  27.3 2.1 copy-start.32
  28.5 2.3 copy-start.37
  28.7 0.7 copy-start.9
  29.5 47.4 %copy-start.17 = (f32[3,1,8]{2,1,0:T(1,128)S(1)}, f32[3,1,8]{2,1,0:T(1,128)}, u32[]{:S(2)}) copy-start(f32[3,1,8]{2,1,0:T(1,128)} %copy-done.16) | copy-start | bytes 292
  29.5 47.4 %copy-start.8 = (bf16[384,512]{1,0:T(8,128)(2,1)S(1)}, bf16[384,512]{1,0:T(8,128)(2,1)}, u32[]{:S(2)}) copy-start(bf16[384,512]{1,0:T(8,128)(2,1)} %param.16) | copy-start | bytes 1179652
  30.0 47.8 %copy-start.19 = (f32[3,1,1,8]{3,2,1,0:T(1,128)S(1)}, f32[3,1,1,8]{3,2,1,0:T(1,128)}, u32[]{:S(2)}) copy-start(f32[3,1,1,8]{3,2,1,0:T(1,128)} %copy-done.18) | copy-start | bytes 292
  30.0 49.2 %copy-start.20 = (f32[3,1,1,8]{3,2,1,0:T(1,128)S(1)}, f32[3,1,1,8]{3,2,1,0:T(1,128)}, u32[]{:S(2)}) copy-start(f32[3,1,1,8]{3,2,1,0:T(1,128)} %get-tuple-element.13) | copy-start | bytes 292
  30.0 49.8 %copy-start.6 = (f32[3,128,8]{2,1,0:T(8,128)S(1)}, f32[3,128,8]{2,1,0:T(8,128)}, u32[]{:S(2)}) copy-start(f32[3,128,8]{2,1,0:T(8,128)} %get-tuple-element.11) | copy-start | bytes 36868
  30.0 69.4 %copy-start.3 = (f32[384,1,128]{2,1,0:T(1,128)S(1)}, f32[384,1,128]{2,1,0:T(1,128)}, u32[]{:S(2)}) copy-start(f32[384,1,128]{2,1,0:T(1,128)} %copy-done.2) | copy-start | bytes 589828
  30.7 86.5 %all-gather.4.cloned.1.call-start = ((), (), s32[]{:S(2)}) async-start(), calls=%async_computation.5 | async-start | bytes 1179648 | tf_op jit(solution)/shard_map/all_gather | solution.py:55
  44.7 54.9 %copy-start.27 = (f32[8]{0:T(128)}, f32[8]{0:T(128)S(1)}, u32[]{:S(2)}) copy-start(f32[8]{0:T(128)S(1)} %get-tuple-element.25) | copy-start | bytes 100
  44.7 54.9 %copy-start.21 = (f32[8]{0:T(128)}, f32[8]{0:T(128)S(1)}, u32[]{:S(2)}) copy-start(f32[8]{0:T(128)S(1)} %get-tuple-element.27) | copy-start | bytes 100
  44.7 54.9 %copy-start.22 = (f32[8]{0:T(128)}, f32[8]{0:T(128)S(1)}, u32[]{:S(2)}) copy-start(f32[8]{0:T(128)S(1)} %get-tuple-element.28) | copy-start | bytes 100
  44.7 54.9 %copy-start.23 = (f32[8]{0:T(128)}, f32[8]{0:T(128)S(1)}, u32[]{:S(2)}) copy-start(f32[8]{0:T(128)S(1)} %get-tuple-element.29) | copy-start | bytes 100
  44.7 54.9 %copy-start.24 = (f32[8]{0:T(128)}, f32[8]{0:T(128)S(1)}, u32[]{:S(2)}) copy-start(f32[8]{0:T(128)S(1)} %get-tuple-element.30) | copy-start | bytes 100
  44.7 54.9 %copy-start.25 = (f32[8]{0:T(128)}, f32[8]{0:T(128)S(1)}, u32[]{:S(2)}) copy-start(f32[8]{0:T(128)S(1)} %get-tuple-element.31) | copy-start | bytes 100
  44.7 54.9 %copy-start.26 = (f32[8]{0:T(128)}, f32[8]{0:T(128)S(1)}, u32[]{:S(2)}) copy-start(f32[8]{0:T(128)S(1)} %get-tuple-element.32) | copy-start | bytes 100
  99.7 17.5 %copy-start.1 = (bf16[64,64,128]{2,1,0:T(8,128)(2,1)S(1)}, bf16[64,64,128]{2,1,0:T(8,128)(2,1)}, u32[]{:S(2)}) copy-start(bf16[64,64,128]{2,1,0:T(8,128)(2,1)} %all-gather.6.cloned.1.call-done) | copy-start | bytes 3145732
  102.6 16.7 %copy-start.33 = (f32[3,8]{0,1:T(8,128)S(1)}, f32[3,8]{0,1:T(8,128)}, u32[]{:S(2)}) copy-start(f32[3,8]{0,1:T(8,128)} %copy.112) | copy-start | bytes 292
  102.6 16.7 %copy-start.34 = (f32[3,8]{0,1:T(8,128)S(1)}, f32[3,8]{0,1:T(8,128)}, u32[]{:S(2)}) copy-start(f32[3,8]{0,1:T(8,128)} %copy.110) | copy-start | bytes 292
  102.6 16.8 %copy-start.35 = (f32[3,1,1,8]{0,3,2,1:T(8,128)S(1)}, f32[3,1,1,8]{0,3,2,1:T(8,128)}, u32[]{:S(2)}) copy-start(f32[3,1,1,8]{0,3,2,1:T(8,128)} %copy.125) | copy-start | bytes 292
  102.6 16.8 %copy-start.39 = (pred[3,3]{1,0:T(4,128)(4,1)S(1)}, pred[3,3]{1,0:T(4,128)(4,1)}, u32[]{:S(2)}) copy-start(pred[3,3]{1,0:T(4,128)(4,1)} %iota_compare_fusion.1) | copy-start | bytes 31
  117.2 2.1 copy-start.10
  119.3 1.1 copy-start.5
  120.4 1.0 copy-start.4
  120.7 1.0 copy-start.38
  148.6 0.9 copy-start.12
  148.6 8.8 %copy-start.36 = (f32[256]{0:T(256)S(1)}, f32[256]{0:T(256)}, u32[]{:S(2)}) copy-start(f32[256]{0:T(256)} %param.25) | copy-start | bytes 3076
  159.1 4.6 %copy-start.14 = (bf16[1024,32]{0,1:T(8,128)(2,1)S(1)}, bf16[1024,32]{0,1:T(8,128)(2,1)}, u32[]{:S(2)}) copy-start(bf16[1024,32]{0,1:T(8,128)(2,1)} %param.27) | copy-start | bytes 196612
  159.1 4.7 %copy-start.15 = (bf16[32,1024]{1,0:T(8,128)(2,1)S(1)}, bf16[32,1024]{1,0:T(8,128)(2,1)}, u32[]{:S(2)}) copy-start(bf16[32,1024]{1,0:T(8,128)(2,1)} %param.26) | copy-start | bytes 196612
  159.1 26.0 %all-to-all-start.2 = ((bf16[8,384,256]{1,2,0:T(8,128)(2,1)}), bf16[8,384,256]{1,2,0:T(8,128)(2,1)}, u32[]{:S(2)}, u32[]{:S(2)}) async-start(bf16[8,384,256]{1,2,0:T(8,128)(2,1)} %broadcast_in_dim.54), calls=%async_computation.2 | async-start | bytes 3145728 | tf_op jit(solution)/shard_map/all_to_all | solution.py:83
Sparse Core Ops, SparseCore 0:
  30.8 43.0 all-gather.5
  76.3 40.9 all-gather.3
